TPU v7x, 32 devices: a whole 2x2x4 slice. The times are simulated.
32 devices in a mesh: sp: 8 (over z, x), tp: 4 (over y, core).
Axes of the slice: x: 2, y: 2, z: 4, core: 2. Of those that a mesh axis runs over, the one named last changes fastest.
Arguments:
- residual: bfloat16 [4096, 2048], P(('sp', 'tp')), may hold values from -6 to 6
- conv_value: bfloat16 [4096, 1024], P('sp', 'tp'), may hold values from -6 to 6
- conv_gate: bfloat16 [4096, 1024], P('sp', 'tp'), may hold values from -9 to 9
- segments: int32 [4096], P('sp'), may hold values from 0 to 3, never falling along the last dimension, each value on 1 to 2048 neighbouring positions
- conv_weight: float32 [31, 1024], P(None, 'tp'), may hold values from -1 to 1
- norm_gain: float32 [1024], P('tp'), may hold values from 0.1 to 1.9
- norm_shift: float32 [1024], P('tp'), may hold values from -3 to 3
- out_weight: bfloat16 [1024, 2048], replicated, may hold values from -0.1875 to 0.1875
- ffn_gain: float32 [2048], replicated, may hold values from 0.1 to 1.9
- routes: int32 [4096, 2], P('sp'), may hold values from 0 to 7, all different within a row; in each aligned block of 128 rows (0 to 127, 128 to 255, ...) at most 64 rows name the same one
- route_weights: float32 [4096, 2], P('sp'), may hold values from 0.2 to 1
- w_gate: bfloat16 [8, 2048, 1024], P('sp', None, 'tp'), may hold values from -0.125 to 0.125
- w_up: bfloat16 [8, 2048, 1024], P('sp', None, 'tp'), may hold values from -0.125 to 0.125
- w_down: bfloat16 [8, 1024, 2048], P('sp', 'tp'), may hold values from -0.1875 to 0.1875
Outputs:
- layer_out: bfloat16 [4096, 2048], P(('sp', 'tp'))
Inputs may be any that keep to these rules, and one draw needn't show every extreme that they name: `routes`: within the rows of one device (aligned blocks of 512 / 4 rows), no expert is named more than 64 times; the two experts of a row differ. `segments`: document numbers never fall along the sequence.
All inputs are finite; a program needn't handle non-finite values.
Results may differ from a plain program's by a relative error of at most 0.007.
Values may be sent and summed in bfloat16 or wider, within the bound.
A program may use at most 128 MiB of HBM per device.

v0:
```python
import jax
import jax.numpy as jnp
from jax import lax
from jax.sharding import PartitionSpec as P

DC = 1024
CONV_GROUPS = 8


def passed_along(value, axis, steps):
    count = lax.axis_size(axis)
    initial, last = (max(0, -steps), min(count, count - steps))
    return lax.ppermute(value, axis, [(source, source + steps) for source in range(initial, last)])


def slot_numbers(block_routes, capacity, experts_n):
    route_pairs = block_routes.reshape(block_routes.shape[:-2] + (-1,))
    onehot = (route_pairs[..., None] == jnp.arange(experts_n, dtype=jnp.int32)).astype(jnp.int32)
    slot_rank = jnp.sum((jnp.cumsum(onehot, axis=-2) - onehot) * onehot, axis=-1)
    return (route_pairs * capacity + slot_rank).reshape(block_routes.shape)


def dispatch_matrix(slot_ids, slot_total):
    numbers = jnp.arange(slot_total, dtype=jnp.int32)[:, None, None]
    matches = jnp.any(numbers == slot_ids[..., None, :, :], axis=-1)
    return matches.astype(jnp.bfloat16)


def shards(
    residual,
    conv_value,
    conv_gate,
    segments,
    conv_weight,
    norm_gain,
    norm_shift,
    out_weight,
    ffn_gain,
    routes,
    route_weights,
    w_gate,
    w_up,
    w_down,
):
    tok_dev, local_channels = conv_value.shape
    reach = conv_weight.shape[0] - 1
    whole_gate, whole_up = (
        lax.all_gather(w_gate[0], "tp", axis=1, tiled=True),
        lax.all_gather(w_up[0], "tp", axis=1, tiled=True),
    )
    whole_down = lax.all_gather(w_down[0], "tp", axis=0, tiled=True)
    gated = (conv_value.astype(jnp.float32) * jax.nn.sigmoid(conv_gate.astype(jnp.float32))).astype(
        jnp.bfloat16
    )
    rim_prev, seg_prev = passed_along(
        (gated[tok_dev - reach :], segments[tok_dev - reach :]), "sp", 1
    )
    extended = jnp.concatenate([rim_prev, gated], 0).astype(jnp.float32)
    seg_ext = jnp.concatenate([seg_prev, segments], 0)
    convolved = jnp.zeros((tok_dev, local_channels), jnp.float32)
    for offset in range(reach + 1):
        same_doc = (seg_ext[offset : offset + tok_dev] == segments)[:, None]
        convolved = convolved + jnp.where(
            same_doc, extended[offset : offset + tok_dev] * conv_weight[offset], 0.0
        )
    group_size = DC // CONV_GROUPS
    grouped = convolved.reshape(tok_dev, local_channels // group_size, group_size)
    group_mean = jnp.mean(grouped, axis=-1, keepdims=True)
    group_var = jnp.mean(jnp.square(grouped - group_mean), axis=-1, keepdims=True)
    scaled = ((grouped - group_mean) * lax.rsqrt(group_var + 1e-05)).reshape(
        tok_dev, local_channels
    ) * norm_gain + norm_shift
    conv_out = jax.nn.silu(scaled).astype(jnp.bfloat16)
    columns = lax.axis_size("tp")
    column = lax.axis_index("tp")
    rows_own = tok_dev // columns
    own_conv = lax.all_to_all(conv_out, "tp", split_axis=0, concat_axis=1, tiled=True)
    mixed = jnp.dot(own_conv, out_weight, preferred_element_type=jnp.float32)
    stream = residual.astype(jnp.float32) + lax.optimization_barrier(
        mixed.astype(jnp.bfloat16)
    ).astype(jnp.float32)
    normed = (
        stream * lax.rsqrt(jnp.mean(stream * stream, axis=-1, keepdims=True) + 1e-06) * ffn_gain
    ).astype(jnp.bfloat16)
    experts_n = lax.axis_size("sp")
    top_count = routes.shape[1]
    model_width = normed.shape[1]
    capacity = max(2, 2 * tok_dev * top_count // (columns * experts_n))
    slot_total = experts_n * capacity
    own_routes = lax.dynamic_slice_in_dim(routes, column * rows_own, rows_own, 0)
    own_weights = lax.dynamic_slice_in_dim(route_weights, column * rows_own, rows_own, 0)
    own_slots = slot_numbers(own_routes, capacity, experts_n)
    routing_table = dispatch_matrix(own_slots, slot_total)
    outgoing = jnp.dot(routing_table, normed, preferred_element_type=jnp.float32).astype(
        jnp.bfloat16
    )
    outgoing = outgoing.reshape(experts_n, capacity, model_width)
    arrived = lax.all_to_all(outgoing, "sp", split_axis=0, concat_axis=1, tiled=True).reshape(
        slot_total, model_width
    )
    gate_act = jnp.dot(arrived, whole_gate, preferred_element_type=jnp.float32)
    up_act = jnp.dot(arrived, whole_up, preferred_element_type=jnp.float32)
    hidden = (jax.nn.silu(gate_act) * up_act).astype(jnp.bfloat16)
    summed = jnp.dot(hidden, whole_down, preferred_element_type=jnp.float32)
    expert_out = summed.astype(jnp.bfloat16).reshape(experts_n, capacity, model_width)
    returned = lax.all_to_all(expert_out, "sp", split_axis=0, concat_axis=0, tiled=True).reshape(
        slot_total, model_width
    )
    combined = stream
    for member in range(top_count):
        chosen = jnp.take(returned, own_slots[:, member], axis=0).astype(jnp.float32)
        combined = combined + own_weights[:, member : member + 1] * chosen
    return combined.astype(jnp.bfloat16)


def solution(mesh):
    return jax.shard_map(
        shards,
        mesh=mesh,
        in_specs=(
            P(("sp", "tp"), None),
            P("sp", "tp"),
            P("sp", "tp"),
            P("sp"),
            P(None, "tp"),
            P("tp"),
            P("tp"),
            P(),
            P(),
            P("sp", None),
            P("sp", None),
            P("sp", None, "tp"),
            P("sp", None, "tp"),
            P("sp", "tp", None),
        ),
        out_specs=P(("sp", "tp"), None),
        check_vma=False,
    )
```

profile of v0, /device:TPU:0, one launch (start us, length us, event | category | flops | bytes accessed | tf_op | source)
XLA Modules:
  0.0 198.8 jit_solution(16494497963675948296)
XLA Ops:
  6.6 0.7 all-gather.7.cloned.1.call-update
  7.3 0.7 all-gather.11.cloned.1.call-update
  8.2 4.9 %collective-permute-start = (s32[30]{0:T(128)S(1)}, s32[30]{0:T(128)S(1)}, u32[]{:S(2)}, u32[]{:S(2)}) collective-permute-start(s32[30]{0:T(128)S(1)} %slice.300), channel_id=1, source_target_pairs={{0,4},{4,8},{8,12},{12,16},{16,20},{20,24},{24,28},{1,5},{5,9},{9,... | collective-permute-start | bytes 368 | tf_op jit(solution)/shard_map/ppermute | solution.py:13
  13.0 0.2 multiply_convert_fusion.4
  13.2 3.5 %collective-permute-start.1 = (bf16[30,256]{1,0:T(8,128)(2,1)S(1)}, bf16[30,256]{1,0:T(8,128)(2,1)S(1)}, u32[]{:S(2)}, u32[]{:S(2)}) collective-permute-start(bf16[30,256]{1,0:T(8,128)(2,1)S(1)} %slice.404), channel_id=1, source_target_pairs={{0,4},{4,8},{8,12},{12,16},{16,20},{20,24},{24,28},{1,5},{5,9},{9,... | collective-permute-start | bytes 46088 | tf_op jit(solution)/shard_map/ppermute | solution.py:13
  17.2 0.6 reduce-window.6
  17.8 0.2 slice_reduce_fusion.2
  18.1 0.1 reduce_sum.41
  18.6 4.0 %fusion.15 = f32[512,256]{1,0:T(8,128)S(1)} fusion(f32[542,256]{1,0:T(8,128)S(1)} %maximum_convert_fusion, f32[256]{0:T(256)S(1)} %bitcast.154, f32[256]{0:T(256)S(1)} %bitcast.156, f32[256]{0:T(256)S(1)} %bitcast.98, f32[256]{0:T(256)S(1)} %bitcast.100, f32[256]{0:T(256)S(1)} %bitcast.102, f32[256]{0:T(256)S(1)} %bitcast.104, f32[256]{0:T(256)S(1)} %bitcast.106, ...), kind=kLoop, calls=%fused_computation.21 | loop fusion | flops 11927552 | bytes 16824320 | tf_op jit(solution)/shard_map/add | solution.py:63
  22.7 0.3 reshape.109
  23.0 0.6 reduce_sum.38
  23.6 1.6 multiply_reduce_fusion.1
  25.3 0.6 mul.492
  25.9 0.6 sub.20
  26.5 5.0 %multiply_convert_fusion.3 = bf16[512,256]{1,0:T(8,128)(2,1)} fusion(f32[64,8,2,128]{3,2,1,0:T(2,128)S(1)} %bitcast.89, f32[64,8,2,128]{3,2,1,0:T(2,128)S(1)} %bitcast.90, f32[256]{0:T(256)S(1)} %copy-done.7, f32[256]{0:T(256)S(1)} %copy-done.8, f32[256]{0:T(256)S(1)} %bitcast.155, f32[542,256]{1,0:T(8,128)S(1)} %maximum_convert_fusion, ...), kind=kLoop, calls=%fused_computation.114 | loop fusion | flops 13107200 | bytes 17612800 | tf_op jit(solution)/shard_map/convert_element_type | solution.py:73
  31.5 3.4 %all-to-all-start = ((bf16[4,128,256]{2,1,0:T(8,128)(2,1)}), bf16[4,128,256]{2,1,0:T(8,128)(2,1)S(1)}, u32[]{:S(2)}, u32[]{:S(2)}) async-start(bf16[4,128,256]{2,1,0:T(8,128)(2,1)} %bitcast.31), calls=%async_computation | async-start | bytes 524288 | tf_op jit(solution)/shard_map/all_to_all | solution.py:77
  35.1 9.0 %all-to-all-done = bf16[4,128,256]{2,1,0:T(8,128)(2,1)S(1)} async-done(((bf16[4,128,256]{2,1,0:T(8,128)(2,1)}), bf16[4,128,256]{2,1,0:T(8,128)(2,1)S(1)}, u32[]{:S(2)}, u32[]{:S(2)}) %all-to-all-start) | async-done | bytes 262176 | tf_op jit(solution)/shard_map/all_to_all | solution.py:77
  44.1 0.2 copy.19
  44.3 3.0 %convolution_convert_fusion.1 = bf16[128,2048]{1,0:T(8,128)(2,1)S(1)} fusion(bf16[128,1024]{0,1:T(8,128)(2,1)S(1)} %bitcast.94, bf16[1024,2048]{1,0:T(8,128)(2,1)} %param.23), kind=kOutput, calls=%fused_computation.10 | convolution fusion | flops 537133056 | bytes 4980736 | tf_op jit(solution)/shard_map/dot_general | solution.py:78
  47.3 0.3 multiply_reduce_fusion
  47.6 0.8 convolution_convert_fusion
  48.4 54.0 %all_to_all.33 = bf16[8,64,2048]{2,1,0:T(8,128)(2,1)S(1)} all-to-all(bf16[8,64,2048]{2,1,0:T(8,128)(2,1)S(1)} %bitcast.88), channel_id=1, replica_groups=mesh['sp'=8,'tp'=4] {'sp'}, dimensions={0} | all-to-all | bytes 4194304 | tf_op jit(solution)/shard_map/all_to_all | solution.py:98
  102.4 5.9 %fusion.4 = f32[512,1024]{1,0:T(8,128)} fusion(bf16[512,2048]{1,0:T(8,128)(2,1)S(1)} %bitcast.92, bf16[1,2048,1024]{2,1,0:T(8,128)(2,1)} %all-gather.7.cloned.1.call-done), kind=kOutput, calls=%fused_computation.6 | convolution fusion | flops 2147483648 | bytes 8388608 | tf_op jit(solution)/shard_map/dot_general | solution.py:101
  108.3 13.8 %all-gather.9.cloned.1.call-done = bf16[1,2048,1024]{2,1,0:T(8,128)(2,1)} async-done(((bf16[1,2048,256]{2,1,0:T(8,128)(2,1)}), bf16[1,2048,1024]{2,1,0:T(8,128)(2,1)}) %all-gather.9.cloned.1.call-update) | async-done | bytes 4194320 | tf_op jit(solution)/shard_map/all_gather | solution.py:49
  122.1 10.0 %fusion.6 = bf16[512,2048]{1,0:T(8,128)(2,1)} fusion(bf16[1,1024,2048]{2,1,0:T(8,128)(2,1)} %all-gather.11.cloned.1.call-done, f32[512,1024]{1,0:T(8,128)} %fusion.4, bf16[512,2048]{1,0:T(8,128)(2,1)S(1)} %bitcast.93, bf16[1,2048,1024]{2,1,0:T(8,128)(2,1)} %all-gather.9.cloned.1.call-done), kind=kOutput, calls=%fused_computation.8 | convolution fusion | flops 4299161600 | bytes 14680064 | tf_op jit(solution)/shard_map/dot_general | solution.py:104
  132.2 5.5 %all-to-all-start.2 = ((bf16[8,64,2048]{2,1,0:T(8,128)(2,1)}), bf16[8,64,2048]{2,1,0:T(8,128)(2,1)S(1)}, u32[]{:S(2)}, u32[]{:S(2)}) async-start(bf16[8,64,2048]{2,1,0:T(8,128)(2,1)} %bitcast.91), calls=%async_computation.2 | async-start | bytes 4194304 | tf_op jit(solution)/shard_map/all_to_all | solution.py:106
  137.7 0.7 constant_dynamic-slice_fusion.1
  138.3 0.2 slice_reduce_fusion.1
  138.6 47.7 %all-to-all-done.2 = bf16[8,64,2048]{2,1,0:T(8,128)(2,1)S(1)} async-done(((bf16[8,64,2048]{2,1,0:T(8,128)(2,1)}), bf16[8,64,2048]{2,1,0:T(8,128)(2,1)S(1)}, u32[]{:S(2)}, u32[]{:S(2)}) %all-to-all-start.2) | async-done | bytes 2097184 | tf_op jit(solution)/shard_map/all_to_all | solution.py:106
  186.3 1.7 gather_fusion
  188.0 1.7 gather_fusion.1
  189.8 2.5 %add_convert_fusion = bf16[128,2048]{1,0:T(8,128)(2,1)} fusion(bf16[128,2048]{1,0:T(8,128)(2,1)S(1)} %convolution_convert_fusion.1, bf16[128,2048]{1,0:T(8,128)(2,1)S(1)} %copy-done.1, bf16[128,2048]{1,0:T(8,128)(2,1)} %gather_fusion.1, bf16[128,2048]{1,0:T(8,128)(2,1)} %gather_fusion, f32[128]{0:T(128)S(1)} %get-tuple-element.70, ...), kind=kLoop, calls=%fused_computation.12 | loop fusion | flops 3145728 | bytes 2622720 | tf_op jit(solution)/shard_map/convert_element_type | solution.py:113
  (53 shorter events, 1.4 us)
Async XLA Ops:
  6.5 10.2 %copy-start = (s32[512,2]{0,1:T(2,128)S(1)}, s32[512,2]{0,1:T(2,128)}, u32[]{:S(2)}) copy-start(s32[512,2]{0,1:T(2,128)} %param.25) | copy-start | bytes 12292
  6.5 1.5 copy-start.5
  6.5 6.5 %copy-start.3 = (bf16[512,256]{1,0:T(8,128)(2,1)S(1)}, bf16[512,256]{1,0:T(8,128)(2,1)}, u32[]{:S(2)}) copy-start(bf16[512,256]{1,0:T(8,128)(2,1)} %param.17) | copy-start | bytes 786436
  6.5 6.5 %copy-start.2 = (bf16[512,256]{1,0:T(8,128)(2,1)S(1)}, bf16[512,256]{1,0:T(8,128)(2,1)}, u32[]{:S(2)}) copy-start(bf16[512,256]{1,0:T(8,128)(2,1)} %param.18) | copy-start | bytes 786436
  6.5 10.2 %copy-start.4 = (f32[31,256]{1,0:T(8,128)S(1)}, f32[31,256]{1,0:T(8,128)}, u32[]{:S(2)}) copy-start(f32[31,256]{1,0:T(8,128)} %param.20) | copy-start | bytes 95236
  6.5 95.9 %all-gather.7.cloned.1.call-start = ((), (), s32[]{:S(2)}) async-start(), calls=%async_computation.3 | async-start | bytes 5242880 | tf_op jit(solution)/shard_map/all_gather | solution.py:48
  7.3 101.0 %all-gather.11.cloned.1.call-start = ((), (), s32[]{:S(2)}) async-start(), calls=%async_computation.5 | async-start | bytes 5242880 | tf_op jit(solution)/shard_map/all_gather | solution.py:51
  8.0 114.1 %all-gather.9.cloned.1.call-start = ((), (), s32[]{:S(2)}) async-start(), calls=%async_computation.4 | async-start | bytes 5242880 | tf_op jit(solution)/shard_map/all_gather | solution.py:49
  8.2 10.1 %collective-permute-start = (s32[30]{0:T(128)S(1)}, s32[30]{0:T(128)S(1)}, u32[]{:S(2)}, u32[]{:S(2)}) collective-permute-start(s32[30]{0:T(128)S(1)} %slice.300), channel_id=1, source_target_pairs={{0,4},{4,8},{8,12},{12,16},{16,20},{20,24},{24,28},{1,5},{5,9},{9,... | collective-permute-start | bytes 368 | tf_op jit(solution)/shard_map/ppermute | solution.py:13
  13.2 5.4 %collective-permute-start.1 = (bf16[30,256]{1,0:T(8,128)(2,1)S(1)}, bf16[30,256]{1,0:T(8,128)(2,1)S(1)}, u32[]{:S(2)}, u32[]{:S(2)}) collective-permute-start(bf16[30,256]{1,0:T(8,128)(2,1)S(1)} %slice.404), channel_id=1, source_target_pairs={{0,4},{4,8},{8,12},{12,16},{16,20},{20,24},{24,28},{1,5},{5,9},{9,... | collective-permute-start | bytes 46088 | tf_op jit(solution)/shard_map/ppermute | solution.py:13
  23.0 3.5 %copy-start.7 = (f32[256]{0:T(256)S(1)}, f32[256]{0:T(256)}, u32[]{:S(2)}) copy-start(f32[256]{0:T(256)} %param.22) | copy-start | bytes 3076
  23.0 3.5 %copy-start.8 = (f32[256]{0:T(256)S(1)}, f32[256]{0:T(256)}, u32[]{:S(2)}) copy-start(f32[256]{0:T(256)} %param.21) | copy-start | bytes 3076
  31.5 12.6 %all-to-all-start = ((bf16[4,128,256]{2,1,0:T(8,128)(2,1)}), bf16[4,128,256]{2,1,0:T(8,128)(2,1)S(1)}, u32[]{:S(2)}, u32[]{:S(2)}) async-start(bf16[4,128,256]{2,1,0:T(8,128)(2,1)} %bitcast.31), calls=%async_computation | async-start | bytes 524288 | tf_op jit(solution)/shard_map/all_to_all | solution.py:77
  44.3 3.0 %copy-start.1 = (bf16[128,2048]{1,0:T(8,128)(2,1)S(1)}, bf16[128,2048]{1,0:T(8,128)(2,1)}, u32[]{:S(2)}) copy-start(bf16[128,2048]{1,0:T(8,128)(2,1)} %param.16) | copy-start | bytes 1572868
  44.3 3.3 %copy-start.6 = (f32[2048]{0:T(1024)S(1)}, f32[2048]{0:T(1024)}, u32[]{:S(2)}) copy-start(f32[2048]{0:T(1024)} %param.24) | copy-start | bytes 24580
  132.2 54.2 %all-to-all-start.2 = ((bf16[8,64,2048]{2,1,0:T(8,128)(2,1)}), bf16[8,64,2048]{2,1,0:T(8,128)(2,1)S(1)}, u32[]{:S(2)}, u32[]{:S(2)}) async-start(bf16[8,64,2048]{2,1,0:T(8,128)(2,1)} %bitcast.91), calls=%async_computation.2 | async-start | bytes 4194304 | tf_op jit(solution)/shard_map/all_to_all | solution.py:106
Sparse Core Ops, SparseCore 0:
  8.9 40.5 all-gather.6
  51.0 34.4 all-gather.10
  87.1 34.9 all-gather.8
where the time goes:
time: 199 us
  waiting for transfers between devices  72 us (36%)
  blocking collectives  54 us (27%)
  matrix products  19.7 us (10%)
  starting transfers between devices  17.3 us (9%)
  other arithmetic  15.3 us (8%)
  between operations  13.5 us (7%)
  local copies, waits for them, and re-layouts  6.92 us (3%)
    all_to_all x1, blocking collectives, shards(): lax.all_to_all(outgoing, 'sp', split_axis=0, concat_axis=1, tiled=True)  54 us
    all_to_all x1, waiting for transfers between devices, shards(): lax.all_to_all(expert_out, 'sp', split_axis=0, concat_axis=0, tiled=True)  47.7 us
    all_gather x1, waiting for transfers between devices, shards(): lax.all_gather(w_up[0], 'tp', axis=1, tiled=True)  13.8 us
    dot_general x1, matrix products, shards(): summed = jnp.dot(hidden, whole_down, preferred_element_type=jnp.float32)  10 us
    all_to_all x1, waiting for transfers between devices, shards(): lax.all_to_all(conv_out, 'tp', split_axis=0, concat_axis=1, tiled=True)  9.03 us
    ppermute x2, starting transfers between devices, passed_along(): lax.ppermute(value, axis, [(source, source + steps) for source in range(i...  8.32 us
    dot_general x1, matrix products, shards(): gate_act = jnp.dot(arrived, whole_gate, preferred_element_type=jnp.float32)  5.89 us
    all_to_all x1, starting transfers between devices, shards(): lax.all_to_all(expert_out, 'sp', split_axis=0, concat_axis=0, tiled=True)  5.51 us
  transfers between devices with their start and end apart: 7, of which 3 were waited for; matrix products, arithmetic and copies ran while one was open for 13% of the time, Pallas kernels for 0%

commit v1 on v0

--- a/solution.py
+++ b/solution.py
@@ -74,7 +74,10 @@
     columns = lax.axis_size("tp")
     column = lax.axis_index("tp")
     rows_own = tok_dev // columns
-    own_conv = lax.all_to_all(conv_out, "tp", split_axis=0, concat_axis=1, tiled=True)
+    n_dev = lax.axis_size("tp")
+    blocks = jnp.stack(jnp.split(conv_out, n_dev, axis=0), axis=0)
+    blocks = lax.all_to_all(blocks, "tp", split_axis=0, concat_axis=0)
+    own_conv = jnp.concatenate(blocks, axis=1)
     mixed = jnp.dot(own_conv, out_weight, preferred_element_type=jnp.float32)
     stream = residual.astype(jnp.float32) + lax.optimization_barrier(
         mixed.astype(jnp.bfloat16)

time: 199 us -> 199 us (level)
  waiting for transfers between devices: 72 us -> 76.5 us
  other arithmetic: 15.3 us -> 11.5 us
    reduce_sum x1, other arithmetic: 0.61 us -> 6.28 us  [shards(): group_mean = jnp.mean(grouped, axis=-1, keepdims=True)]
    convert_element_type x1, other arithmetic: 4.99 us -> 0.25 us  [shards(): conv_out = jax.nn.silu(scaled).astype(jnp.bfloat16)]
    all_gather x1, waiting for transfers between devices: 13.8 us -> 18.3 us  [shards(): lax.all_gather(w_up[0], 'tp', axis=1, tiled=True)]
    add x1 -> x0, other arithmetic: 4.03 us -> none  [shards(): convolved + jnp.where(same_doc, extended[offset:offset + tok_dev] * conv_...]
  transfers between devices with their start and end apart: 7 -> 7, of which waited for: 3 -> 3; matrix products, arithmetic and copies ran while one was open for 13% -> 11% of each run, Pallas kernels for 0% -> 0%
where the time goes in v1:
time: 199 us
  waiting for transfers between devices  76.5 us (38%)
  blocking collectives  54.5 us (27%)
  matrix products  19.8 us (10%)
  starting transfers between devices  17.3 us (9%)
  between operations  13.5 us (7%)
  other arithmetic  11.5 us (6%)
  local copies, waits for them, and re-layouts  5.69 us (3%)
    all_to_all x1, blocking collectives, shards(): lax.all_to_all(outgoing, 'sp', split_axis=0, concat_axis=1, tiled=True)  54.5 us
    all_to_all x1, waiting for transfers between devices, shards(): lax.all_to_all(expert_out, 'sp', split_axis=0, concat_axis=0, tiled=True)  47.7 us
    all_gather x1, waiting for transfers between devices, shards(): lax.all_gather(w_up[0], 'tp', axis=1, tiled=True)  18.3 us
    dot_general x1, matrix products, shards(): summed = jnp.dot(hidden, whole_down, preferred_element_type=jnp.float32)  10 us
    all_to_all x1, waiting for transfers between devices, shards(): blocks = lax.all_to_all(blocks, 'tp', split_axis=0, concat_axis=0)  9.04 us
    ppermute x2, starting transfers between devices, passed_along(): lax.ppermute(value, axis, [(source, source + steps) for source in range(i...  8.32 us
    reduce_sum x1, other arithmetic, shards(): group_mean = jnp.mean(grouped, axis=-1, keepdims=True)  6.28 us
    dot_general x1, matrix products, shards(): gate_act = jnp.dot(arrived, whole_gate, preferred_element_type=jnp.float32)  5.98 us
  transfers between devices with their start and end apart: 7, of which 3 were waited for; matrix products, arithmetic and copies ran while one was open for 11% of the time, Pallas kernels for 0%

profile of v1, /device:TPU:0, one launch (start us, length us, event | category | flops | bytes accessed | tf_op | source)
XLA Modules:
  0.0 198.8 jit_solution(11046535242621036208)
XLA Ops:
  6.6 0.7 all-gather.7.cloned.1.call-update
  7.3 0.7 all-gather.11.cloned.1.call-update
  8.2 4.9 %collective-permute-start = (s32[30]{0:T(128)S(1)}, s32[30]{0:T(128)S(1)}, u32[]{:S(2)}, u32[]{:S(2)}) collective-permute-start(s32[30]{0:T(128)S(1)} %slice.300), channel_id=1, source_target_pairs={{0,4},{4,8},{8,12},{12,16},{16,20},{20,24},{24,28},{1,5},{5,9},{9,... | collective-permute-start | bytes 368 | tf_op jit(solution)/shard_map/ppermute | solution.py:13
  13.0 0.1 copy.22
  13.2 0.1 copy.23
  13.3 0.1 multiply_convert_fusion.4
  13.6 3.5 %collective-permute-start.1 = (bf16[30,256]{0,1:T(8,128)(2,1)S(1)}, bf16[30,256]{0,1:T(8,128)(2,1)S(1)}, u32[]{:S(2)}, u32[]{:S(2)}) collective-permute-start(bf16[30,256]{0,1:T(8,128)(2,1)S(1)} %slice.404), channel_id=1, source_target_pairs={{0,4},{4,8},{8,12},{12,16},{16,20},{20,24},{24,28},{1,5},{5,9},{9,... | collective-permute-start | bytes 46088 | tf_op jit(solution)/shard_map/ppermute | solution.py:13
  17.3 0.1 eq.163
  17.4 0.1 eq.159
  17.6 0.6 reduce-window.6
  18.2 0.2 slice_reduce_fusion.2
  18.5 0.1 reduce_sum.41
  19.0 0.2 maximum_convert_fusion
  19.1 6.3 %bitcast_reduce_fusion = (f32[512,2]{0,1:T(2,128)S(1)}, f32[512,256]{0,1:T(8,128)S(1)}) fusion(f32[256]{0:T(256)S(1)} %bitcast.135, f32[542,256]{0,1:T(8,128)S(1)} %maximum_convert_fusion, f32[256]{0:T(256)S(1)} %bitcast.136, pred[512]{0:T(512)(128)(4,1)S(1)} %get-tuple-element.73, f32[256]{0:T(256)S(1)} %bitcast.107, ...), kind=kLoop, calls=%fused_computation.112 | loop fusion | flops 12057600 | bytes 16828416 | tf_op jit(solution)/shard_map/reduce_sum | solution.py:68
  25.6 0.2 multiply_convert_fusion.3
  25.9 0.7 pad_maximum_fusion
  26.6 3.4 %all-to-all-start = ((bf16[4,128,256]{1,2,0:T(8,128)(2,1)}), bf16[4,128,256]{1,2,0:T(8,128)(2,1)S(1)}, u32[]{:S(2)}, u32[]{:S(2)}) async-start(bf16[4,128,256]{1,2,0:T(8,128)(2,1)} %pad_maximum_fusion), calls=%async_computation | async-start | bytes 524288 | tf_op jit(solution)/shard_map/all_to_all | solution.py:79
  30.2 9.0 %all-to-all-done = bf16[4,128,256]{1,2,0:T(8,128)(2,1)S(1)} async-done(((bf16[4,128,256]{1,2,0:T(8,128)(2,1)}), bf16[4,128,256]{1,2,0:T(8,128)(2,1)S(1)}, u32[]{:S(2)}, u32[]{:S(2)}) %all-to-all-start) | async-done | bytes 262176 | tf_op jit(solution)/shard_map/all_to_all | solution.py:79
  39.2 3.0 %convolution_convert_fusion.1 = bf16[128,2048]{1,0:T(8,128)(2,1)S(1)} fusion(bf16[128,1024]{0,1:T(8,128)(2,1)S(1)} %bitcast.105, bf16[1024,2048]{1,0:T(8,128)(2,1)} %param.23), kind=kOutput, calls=%fused_computation.10 | convolution fusion | flops 537133056 | bytes 4980736 | tf_op jit(solution)/shard_map/dot_general | solution.py:81
  42.2 0.3 multiply_reduce_fusion
  42.5 0.8 convolution_convert_fusion
  43.3 54.5 %all_to_all.19 = bf16[8,64,2048]{2,1,0:T(8,128)(2,1)S(1)} all-to-all(bf16[8,64,2048]{2,1,0:T(8,128)(2,1)S(1)} %bitcast.101), channel_id=1, replica_groups=mesh['sp'=8,'tp'=4] {'sp'}, dimensions={0} | all-to-all | bytes 4194304 | tf_op jit(solution)/shard_map/all_to_all | solution.py:101
  97.8 6.0 %fusion.4 = f32[512,1024]{1,0:T(8,128)} fusion(bf16[512,2048]{1,0:T(8,128)(2,1)S(1)} %bitcast.103, bf16[1,2048,1024]{2,1,0:T(8,128)(2,1)} %all-gather.7.cloned.1.call-done), kind=kOutput, calls=%fused_computation.6 | convolution fusion | flops 2147483648 | bytes 8388608 | tf_op jit(solution)/shard_map/dot_general | solution.py:104
  103.8 18.3 %all-gather.9.cloned.1.call-done = bf16[1,2048,1024]{2,1,0:T(8,128)(2,1)} async-done(((bf16[1,2048,256]{2,1,0:T(8,128)(2,1)}), bf16[1,2048,1024]{2,1,0:T(8,128)(2,1)}) %all-gather.9.cloned.1.call-update) | async-done | bytes 4194320 | tf_op jit(solution)/shard_map/all_gather | solution.py:49
  122.1 10.0 %fusion.6 = bf16[512,2048]{1,0:T(8,128)(2,1)} fusion(bf16[1,1024,2048]{2,1,0:T(8,128)(2,1)} %all-gather.11.cloned.1.call-done, f32[512,1024]{1,0:T(8,128)} %fusion.4, bf16[512,2048]{1,0:T(8,128)(2,1)S(1)} %bitcast.104, bf16[1,2048,1024]{2,1,0:T(8,128)(2,1)} %all-gather.9.cloned.1.call-done), kind=kOutput, calls=%fused_computation.8 | convolution fusion | flops 4299161600 | bytes 14680064 | tf_op jit(solution)/shard_map/dot_general | solution.py:107
  132.1 5.5 %all-to-all-start.2 = ((bf16[8,64,2048]{2,1,0:T(8,128)(2,1)}), bf16[8,64,2048]{2,1,0:T(8,128)(2,1)S(1)}, u32[]{:S(2)}, u32[]{:S(2)}) async-start(bf16[8,64,2048]{2,1,0:T(8,128)(2,1)} %bitcast.102), calls=%async_computation.2 | async-start | bytes 4194304 | tf_op jit(solution)/shard_map/all_to_all | solution.py:109
  137.6 0.7 constant_dynamic-slice_fusion.1
  138.3 0.2 slice_reduce_fusion.1
  138.5 47.7 %all-to-all-done.2 = bf16[8,64,2048]{2,1,0:T(8,128)(2,1)S(1)} async-done(((bf16[8,64,2048]{2,1,0:T(8,128)(2,1)}), bf16[8,64,2048]{2,1,0:T(8,128)(2,1)S(1)}, u32[]{:S(2)}, u32[]{:S(2)}) %all-to-all-start.2) | async-done | bytes 2097184 | tf_op jit(solution)/shard_map/all_to_all | solution.py:109
  186.3 1.7 gather_fusion
  188.0 1.7 gather_fusion.1
  189.7 2.5 %add_convert_fusion = bf16[128,2048]{1,0:T(8,128)(2,1)} fusion(bf16[128,2048]{1,0:T(8,128)(2,1)S(1)} %convolution_convert_fusion.1, bf16[128,2048]{1,0:T(8,128)(2,1)S(1)} %copy-done.1, bf16[128,2048]{1,0:T(8,128)(2,1)} %gather_fusion.1, bf16[128,2048]{1,0:T(8,128)(2,1)} %gather_fusion, f32[128]{0:T(128)S(1)} %get-tuple-element.76, ...), kind=kLoop, calls=%fused_computation.12 | loop fusion | flops 3145728 | bytes 2622720 | tf_op jit(solution)/shard_map/convert_element_type | solution.py:116
  (52 shorter events, 1.2 us)
Async XLA Ops:
  6.5 10.6 %copy-start = (s32[512,2]{0,1:T(2,128)S(1)}, s32[512,2]{0,1:T(2,128)}, u32[]{:S(2)}) copy-start(s32[512,2]{0,1:T(2,128)} %param.25) | copy-start | bytes 12292
  6.5 1.5 copy-start.5
  6.5 6.5 %copy-start.2 = (bf16[512,256]{1,0:T(8,128)(2,1)S(1)}, bf16[512,256]{1,0:T(8,128)(2,1)}, u32[]{:S(2)}) copy-start(bf16[512,256]{1,0:T(8,128)(2,1)} %param.17) | copy-start | bytes 786436
  6.5 6.6 %copy-start.3 = (bf16[512,256]{1,0:T(8,128)(2,1)S(1)}, bf16[512,256]{1,0:T(8,128)(2,1)}, u32[]{:S(2)}) copy-start(bf16[512,256]{1,0:T(8,128)(2,1)} %param.18) | copy-start | bytes 786436
  6.5 91.3 %all-gather.7.cloned.1.call-start = ((), (), s32[]{:S(2)}) async-start(), calls=%async_computation.3 | async-start | bytes 5242880 | tf_op jit(solution)/shard_map/all_gather | solution.py:48
  7.3 9.8 %copy-start.4 = (f32[31,256]{1,0:T(8,128)S(1)}, f32[31,256]{1,0:T(8,128)}, u32[]{:S(2)}) copy-start(f32[31,256]{1,0:T(8,128)} %param.20) | copy-start | bytes 95236
  7.3 96.5 %all-gather.11.cloned.1.call-start = ((), (), s32[]{:S(2)}) async-start(), calls=%async_computation.5 | async-start | bytes 5242880 | tf_op jit(solution)/shard_map/all_gather | solution.py:51
  8.0 114.1 %all-gather.9.cloned.1.call-start = ((), (), s32[]{:S(2)}) async-start(), calls=%async_computation.4 | async-start | bytes 5242880 | tf_op jit(solution)/shard_map/all_gather | solution.py:49
  8.2 10.5 %collective-permute-start = (s32[30]{0:T(128)S(1)}, s32[30]{0:T(128)S(1)}, u32[]{:S(2)}, u32[]{:S(2)}) collective-permute-start(s32[30]{0:T(128)S(1)} %slice.300), channel_id=1, source_target_pairs={{0,4},{4,8},{8,12},{12,16},{16,20},{20,24},{24,28},{1,5},{5,9},{9,... | collective-permute-start | bytes 368 | tf_op jit(solution)/shard_map/ppermute | solution.py:13
  13.6 5.4 %collective-permute-start.1 = (bf16[30,256]{0,1:T(8,128)(2,1)S(1)}, bf16[30,256]{0,1:T(8,128)(2,1)S(1)}, u32[]{:S(2)}, u32[]{:S(2)}) collective-permute-start(bf16[30,256]{0,1:T(8,128)(2,1)S(1)} %slice.404), channel_id=1, source_target_pairs={{0,4},{4,8},{8,12},{12,16},{16,20},{20,24},{24,28},{1,5},{5,9},{9,... | collective-permute-start | bytes 46088 | tf_op jit(solution)/shard_map/ppermute | solution.py:13
  19.1 6.4 %copy-start.7 = (f32[256]{0:T(256)S(1)}, f32[256]{0:T(256)}, u32[]{:S(2)}) copy-start(f32[256]{0:T(256)} %param.22) | copy-start | bytes 3076
  19.1 6.4 %copy-start.8 = (f32[256]{0:T(256)S(1)}, f32[256]{0:T(256)}, u32[]{:S(2)}) copy-start(f32[256]{0:T(256)} %param.21) | copy-start | bytes 3076
  26.6 12.6 %all-to-all-start = ((bf16[4,128,256]{1,2,0:T(8,128)(2,1)}), bf16[4,128,256]{1,2,0:T(8,128)(2,1)S(1)}, u32[]{:S(2)}, u32[]{:S(2)}) async-start(bf16[4,128,256]{1,2,0:T(8,128)(2,1)} %pad_maximum_fusion), calls=%async_computation | async-start | bytes 524288 | tf_op jit(solution)/shard_map/all_to_all | solution.py:79
  39.2 3.0 %copy-start.1 = (bf16[128,2048]{1,0:T(8,128)(2,1)S(1)}, bf16[128,2048]{1,0:T(8,128)(2,1)}, u32[]{:S(2)}) copy-start(bf16[128,2048]{1,0:T(8,128)(2,1)} %param.16) | copy-start | bytes 1572868
  39.2 3.3 %copy-start.6 = (f32[2048]{0:T(1024)S(1)}, f32[2048]{0:T(1024)}, u32[]{:S(2)}) copy-start(f32[2048]{0:T(1024)} %param.24) | copy-start | bytes 24580
  132.1 54.2 %all-to-all-start.2 = ((bf16[8,64,2048]{2,1,0:T(8,128)(2,1)}), bf16[8,64,2048]{2,1,0:T(8,128)(2,1)S(1)}, u32[]{:S(2)}, u32[]{:S(2)}) async-start(bf16[8,64,2048]{2,1,0:T(8,128)(2,1)} %bitcast.102), calls=%async_computation.2 | async-start | bytes 4194304 | tf_op jit(solution)/shard_map/all_to_all | solution.py:109
Sparse Core Ops, SparseCore 0:
  8.9 40.5 all-gather.6
  51.0 34.4 all-gather.10
  87.1 34.9 all-gather.8
